TPU v7x, 32 devices: a whole 2x2x4 slice. The times are simulated.
32 devices in a mesh: kv: 8 (over z, y), tp: 4 (over x, core).
Axes of the slice: x: 2, y: 2, z: 4, core: 2. Of those that a mesh axis runs over, the one named last changes fastest.
Arguments:
- block_in: bfloat16 [64, 4096], P(None, ('kv', 'tp')), may hold values from -30 to 30
- before_gain: bfloat16 [4096], P('kv'), may hold values from 0.099609375 to 1.8984375
- before_gate: bfloat16 [4096, 11264], P('kv', 'tp'), may hold values from -0.09375 to 0.09375
- before_up: bfloat16 [4096, 11264], P('kv', 'tp'), may hold values from -0.09375 to 0.09375
- before_down: bfloat16 [11264, 4096], P('tp', 'kv'), may hold values from -0.0546875 to 0.0546875
- mix_gain: bfloat16 [4096], P('kv'), may hold values from 0.099609375 to 1.8984375
- input_gate: bfloat16 [4096, 8192], P('kv', 'tp'), may hold values from -0.09375 to 0.09375
- input_value: bfloat16 [4096, 8192], P('kv', 'tp'), may hold values from -0.09375 to 0.09375
- input_write: bfloat16 [4096, 2048], P('kv', 'tp'), may hold values from -0.09375 to 0.09375
- input_read: bfloat16 [4096, 2048], P('kv', 'tp'), may hold values from -0.09375 to 0.09375
- input_step: bfloat16 [4096, 128], P('kv', 'tp'), may hold values from -0.09375 to 0.09375
- step_bias: float32 [128], P('tp'), may hold values from -3 to 0
- decay_log: float32 [128], P('tp'), may hold values from -1 to 1.4
- skip_gain: float32 [128], P('tp'), may hold values from 0.5 to 2
- value_taps: bfloat16 [4, 8192], P(None, 'tp'), may hold values from -3 to 3
- write_taps: bfloat16 [4, 2048], P(None, 'tp'), may hold values from -3 to 3
- read_taps: bfloat16 [4, 2048], P(None, 'tp'), may hold values from -3 to 3
- value_window: bfloat16 [64, 3, 8192], P('kv', None, 'tp'), may hold values from -6 to 6
- write_window: bfloat16 [64, 3, 2048], P('kv', None, 'tp'), may hold values from -6 to 6
- read_window: bfloat16 [64, 3, 2048], P('kv', None, 'tp'), may hold values from -6 to 6
- scan_state: float32 [64, 128, 64, 128], P('kv', 'tp'), may hold values from -2 to 2
- group_gain: bfloat16 [8192], P('tp'), may hold values from 0.099609375 to 1.8984375
- mixer_out: bfloat16 [8192, 4096], P('tp', 'kv'), may hold values from -0.0625 to 0.0625
- after_gain: bfloat16 [4096], P('kv'), may hold values from 0.099609375 to 1.8984375
- after_gate: bfloat16 [4096, 11264], P('kv', 'tp'), may hold values from -0.09375 to 0.09375
- after_up: bfloat16 [4096, 11264], P('kv', 'tp'), may hold values from -0.09375 to 0.09375
- after_down: bfloat16 [11264, 4096], P('tp', 'kv'), may hold values from -0.0546875 to 0.0546875
Outputs:
- block_out: bfloat16 [64, 4096], P(None, ('kv', 'tp'))
- state_next: float32 [64, 128, 64, 128], P('kv', 'tp')
- value_next: bfloat16 [64, 3, 8192], P('kv', None, 'tp')
- write_next: bfloat16 [64, 3, 2048], P('kv', None, 'tp')
- read_next: bfloat16 [64, 3, 2048], P('kv', None, 'tp')
All inputs are finite; a program needn't handle non-finite values.
Results may differ from a plain program's by a relative error of at most 0.0085.
Values may be sent and summed in bfloat16 or wider, within the bound.
A program may use at most 128 MiB of HBM per device.

v0:
```python
import jax
import jax.numpy as jnp
from jax import lax
from jax.sharding import PartitionSpec as P

D = 4096
HEAD_DIM = 64
STATE = 128


EPS = 1e-06


def lifted_rows(current, gain_vec):
    gathered = lax.all_gather(current, "tp", axis=1, tiled=True)
    widened = gathered.astype(jnp.float32)
    squares = jnp.sum(widened * widened, axis=1)
    lifted = (widened * gain_vec.astype(jnp.float32)[None, :]).astype(jnp.bfloat16)
    return (lifted, squares)


def column_sums(partial_terms):
    return lax.psum_scatter(partial_terms, "tp", scatter_dimension=1, tiled=True)


def half_channel(current, gain_vec, gate_weight, up_weight, down_weight):
    lifted, squares = lifted_rows(current, gain_vec)
    gate_part = jnp.dot(lifted, gate_weight, preferred_element_type=jnp.float32)
    up_part = jnp.dot(lifted, up_weight, preferred_element_type=jnp.float32)
    gate_sum, up_sum, totals = lax.psum((gate_part, up_part, squares), "kv")
    row_scale = lax.rsqrt(totals / D + EPS)[:, None]
    hidden = (jax.nn.silu(gate_sum * row_scale) * (up_sum * row_scale)).astype(jnp.bfloat16)
    down_sum = jnp.dot(hidden, down_weight, preferred_element_type=jnp.float32)
    returned = column_sums(down_sum)
    return (current.astype(jnp.float32) + 0.5 * returned).astype(jnp.bfloat16)


def short_conv(window_state, fresh, taps):
    window = jnp.concatenate([window_state, fresh[:, None, :]], axis=1)
    conv_sum = jnp.sum(window.astype(jnp.float32) * taps.astype(jnp.float32)[None], axis=1)
    return (jax.nn.silu(conv_sum), window[:, 1:])


def spread_groups(vectors, heads):
    count = vectors.shape[0]
    groups = vectors.shape[1] // STATE
    shaped = vectors.reshape(count, groups, 1, STATE)
    return jnp.broadcast_to(shaped, (count, groups, heads // groups, STATE)).reshape(
        count, heads, STATE
    )


def state_update(
    gate_rows,
    value_conv,
    write_conv,
    read_conv,
    step_raw,
    step_bias,
    decay_log,
    skip_gain,
    scan_state,
):
    count = value_conv.shape[0]
    heads = step_bias.shape[0]
    step_size = jax.nn.softplus(step_raw + step_bias[None, :])
    decay = jnp.exp(-step_size * jnp.exp(decay_log)[None, :])
    value_heads = value_conv.reshape(count, heads, HEAD_DIM)
    write_heads = spread_groups(write_conv, heads)
    read_heads = spread_groups(read_conv, heads)
    state_next = (
        decay[:, :, None, None] * scan_state
        + (step_size[:, :, None] * value_heads)[:, :, :, None] * write_heads[:, :, None, :]
    )
    readout = (
        jnp.sum(state_next * read_heads[:, :, None, :], axis=3)
        + skip_gain[None, :, None] * value_heads
    )
    gated = readout.reshape(count, heads * HEAD_DIM) * jax.nn.silu(gate_rows.astype(jnp.float32))
    groups = write_conv.shape[1] // STATE
    grouped = gated.reshape(count, groups, heads * HEAD_DIM // groups)
    grouped = grouped * lax.rsqrt(jnp.mean(grouped * grouped, axis=2, keepdims=True) + EPS)
    return (grouped.reshape(count, heads * HEAD_DIM), state_next)


def local(
    block_in,
    before_gain,
    before_gate,
    before_up,
    before_down,
    mix_gain,
    input_gate,
    input_value,
    input_write,
    input_read,
    input_step,
    step_bias,
    decay_log,
    skip_gain,
    value_taps,
    write_taps,
    read_taps,
    value_window,
    write_window,
    read_window,
    scan_state,
    group_gain,
    mixer_out,
    after_gain,
    after_gate,
    after_up,
    after_down,
):
    first_out = half_channel(block_in, before_gain, before_gate, before_up, before_down)
    lifted, squares = lifted_rows(first_out, mix_gain)
    gate_part = jnp.dot(lifted, input_gate, preferred_element_type=jnp.float32)
    value_part = jnp.dot(lifted, input_value, preferred_element_type=jnp.float32)
    write_part = jnp.dot(lifted, input_write, preferred_element_type=jnp.float32)
    read_part = jnp.dot(lifted, input_read, preferred_element_type=jnp.float32)
    step_part = jnp.dot(lifted, input_step, preferred_element_type=jnp.float32)
    gate_sum, value_sum, write_sum, read_sum, step_sum, totals = (
        lax.psum_scatter(gate_part, "kv", scatter_dimension=0, tiled=True),
        lax.psum_scatter(value_part, "kv", scatter_dimension=0, tiled=True),
        lax.psum_scatter(write_part, "kv", scatter_dimension=0, tiled=True),
        lax.psum_scatter(read_part, "kv", scatter_dimension=0, tiled=True),
        lax.psum_scatter(step_part, "kv", scatter_dimension=0, tiled=True),
        lax.psum_scatter(squares, "kv", scatter_dimension=0, tiled=True),
    )
    mix_scale = lax.rsqrt(totals / D + EPS)[:, None]
    gate_rows = (gate_sum * mix_scale).astype(jnp.bfloat16)
    value_fresh = (value_sum * mix_scale).astype(jnp.bfloat16)
    write_fresh = (write_sum * mix_scale).astype(jnp.bfloat16)
    read_fresh = (read_sum * mix_scale).astype(jnp.bfloat16)
    step_raw = step_sum * mix_scale
    value_conv, value_next = short_conv(value_window, value_fresh, value_taps)
    write_conv, write_next = short_conv(write_window, write_fresh, write_taps)
    read_conv, read_next = short_conv(read_window, read_fresh, read_taps)
    normed, state_next = state_update(
        gate_rows,
        value_conv,
        write_conv,
        read_conv,
        step_raw,
        step_bias,
        decay_log,
        skip_gain,
        scan_state,
    )
    mixer_rows = (normed * group_gain.astype(jnp.float32)[None, :]).astype(jnp.bfloat16)
    back_part = jnp.dot(
        lax.all_gather(mixer_rows, "kv", axis=0, tiled=True),
        mixer_out,
        preferred_element_type=jnp.float32,
    )
    returned = column_sums(back_part)
    middle = (first_out.astype(jnp.float32) + returned).astype(jnp.bfloat16)
    block_out = half_channel(middle, after_gain, after_gate, after_up, after_down)
    return (block_out, state_next, value_next, write_next, read_next)


def solution(mesh):
    placed = (
        P(None, ("kv", "tp")),
        P("kv"),
        P("kv", "tp"),
        P("kv", "tp"),
        P("tp", "kv"),
        P("kv"),
        P("kv", "tp"),
        P("kv", "tp"),
        P("kv", "tp"),
        P("kv", "tp"),
        P("kv", "tp"),
        P("tp"),
        P("tp"),
        P("tp"),
        P(None, "tp"),
        P(None, "tp"),
        P(None, "tp"),
        P("kv", None, "tp"),
        P("kv", None, "tp"),
        P("kv", None, "tp"),
        P("kv", "tp", None, None),
        P("tp"),
        P("tp", "kv"),
        P("kv"),
        P("kv", "tp"),
        P("kv", "tp"),
        P("tp", "kv"),
    )
    return jax.shard_map(
        local,
        mesh=mesh,
        in_specs=placed,
        out_specs=(
            P(None, ("kv", "tp")),
            P("kv", "tp", None, None),
            P("kv", None, "tp"),
            P("kv", None, "tp"),
            P("kv", None, "tp"),
        ),
        check_vma=False,
    )
```

profile of v0, /device:TPU:0, one launch (start us, length us, event | category | flops | bytes accessed | tf_op | source)
XLA Modules:
  0.0 575.5 jit_solution(16134604495972762844)
XLA Ops:
  7.2 6.6 %all_gather.12 = bf16[64,512]{1,0:T(8,128)(2,1)S(1)} all-gather(bf16[64,128]{1,0:T(8,128)(2,1)} %param.27), channel_id=1, replica_groups=mesh['kv'=8,'tp'=4] {'tp'}, dimensions={1}, use_global_device_ids=true | all-gather | bytes 81920 | tf_op jit(solution)/shard_map/all_gather | solution.py:15
  17.6 22.7 %psum.43 = f32[64]{0:T(128)S(1)} all-reduce(f32[64]{0:T(128)S(1)} %fusion.7), channel_id=1, replica_groups=mesh['kv'=8,'tp'=4] {'kv'}, use_global_device_ids=true, to_apply=%region_2.0 | all-reduce | flops 64 | bytes 512 | tf_op jit(solution)/shard_map/psum | solution.py:30
  40.4 66.0 %all-reduce.10.cloned.1.call-done = (f32[64,2816]{1,0:T(8,128)}, f32[64,2816]{1,0:T(8,128)}) async-done(((f32[64,2816]{1,0:T(8,128)}, f32[64,2816]{1,0:T(8,128)}), (f32[64,2816]{1,0:T(8,128)}, f32[64,2816]{1,0:T(8,128)})) %all-reduce.10.cloned.1.call-update) | async-done | bytes 1441808 | tf_op jit(solution)/shard_map/psum | solution.py:30
  106.4 3.6 fusion
  110.1 18.8 %reduce-scatter.8.cloned.1.call-done = f32[64,128]{1,0:T(8,128)} async-done(((f32[64,512]{1,0:T(8,128)}), f32[64,128]{1,0:T(8,128)}) %reduce-scatter.8.cloned.1.call-update) | async-done | bytes 32784 | tf_op jit(solution)/shard_map/reduce_scatter | solution.py:23
  129.8 5.3 all_gather.13
  135.9 1.9 fusion.28
  137.9 2.9 fusion.32
  147.2 37.5 %all-reduce.2 = (f32[64]{0:T(128)S(1)}, f32[64,32]{1,0:T(8,128)S(1)}) all-reduce(f32[64]{0:T(128)S(1)} %fusion.9, f32[64,32]{1,0:T(8,128)S(1)} %fusion.34), channel_id=4, replica_groups=mesh['kv'=8,'tp'=4] {'kv'}, use_global_device_ids=true, to_apply=%region_7.8.clone | all-reduce | flops 2112 | bytes 16896
  184.8 2.9 fusion.26
  188.4 9.5 %reduce-scatter.12.cloned.1.call-done = f32[8,512]{1,0:T(8,128)} async-done(((f32[64,512]{1,0:T(8,128)}), f32[8,512]{1,0:T(8,128)}) %reduce-scatter.12.cloned.1.call-update) | async-done | bytes 16400 | tf_op jit(solution)/shard_map/reduce_scatter | solution.py:125
  197.9 64.1 %reduce-scatter.14.cloned.1.call-done = f32[8,512]{1,0:T(8,128)} async-done(((f32[64,512]{1,0:T(8,128)}), f32[8,512]{1,0:T(8,128)}) %reduce-scatter.14.cloned.1.call-update) | async-done | bytes 16400 | tf_op jit(solution)/shard_map/reduce_scatter | solution.py:126
  263.0 64.4 %reduce-scatter.10.cloned.1.call-done = f32[8,2048]{1,0:T(8,128)} async-done(((f32[64,2048]{1,0:T(8,128)}), f32[8,2048]{1,0:T(8,128)}) %reduce-scatter.10.cloned.1.call-update) | async-done | bytes 65552 | tf_op jit(solution)/shard_map/reduce_scatter | solution.py:124
  329.3 9.4 %multiply_reduce_fusion = (f32[8,32,64]{2,1,0:T(8,128)S(1)}, f32[8,32,64,128]{3,2,1,0:T(8,128)}) fusion(f32[8,32,128]{2,1,0:T(8,128)S(1)} %broadcast_bitcast_fusion, f32[8,32,128]{2,1,0:T(8,128)S(1)} %broadcast_bitcast_fusion.1, f32[8,32,64]{2,1,0:T(8,128)S(1)} %multiply_multiply_fusion, f32[8,32,64,128]{3,2,1,0:T(8,128)} %param.47, f32[8,32]{1,0:T(8,128)} %get-tuple-element.15), kind=kLoop, calls=%fused_computation | loop fusion | flops 10469376 | bytes 17171456 | tf_op jit(solution)/shard_map/reduce_sum | solution.py:76
  338.7 53.9 %reduce-scatter.16.cloned.1.call-done = f32[8,2048]{1,0:T(8,128)} async-done(((f32[64,2048]{1,0:T(8,128)}), f32[8,2048]{1,0:T(8,128)}) %reduce-scatter.16.cloned.1.call-update) | async-done | bytes 65552 | tf_op jit(solution)/shard_map/reduce_scatter | solution.py:123
  394.5 30.9 %all_gather.14 = bf16[64,2048]{1,0:T(8,128)(2,1)S(1)} all-gather(bf16[8,2048]{1,0:T(8,128)(2,1)S(1)} %multiply_convert_fusion.4), channel_id=1, replica_groups=mesh['kv'=8,'tp'=4] {'kv'}, dimensions={0}, use_global_device_ids=true | all-gather | bytes 294912 | tf_op jit(solution)/shard_map/all_gather | solution.py:152
  425.4 2.7 fusion.47
  428.2 18.7 %reduce-scatter.18.cloned.1.call-done = f32[64,128]{1,0:T(8,128)} async-done(((f32[64,512]{1,0:T(8,128)}), f32[64,128]{1,0:T(8,128)}) %reduce-scatter.18.cloned.1.call-update) | async-done | bytes 32784 | tf_op jit(solution)/shard_map/reduce_scatter | solution.py:23
  447.8 5.3 all_gather.15
  453.1 3.3 fusion.17
  458.1 22.0 %psum.46 = f32[64]{0:T(128)S(1)} all-reduce(f32[64]{0:T(128)S(1)} %fusion.11), channel_id=1, replica_groups=mesh['kv'=8,'tp'=4] {'kv'}, use_global_device_ids=true, to_apply=%region_20.21 | all-reduce | flops 64 | bytes 512 | tf_op jit(solution)/shard_map/psum | solution.py:30
  480.1 65.0 %all-reduce.8.cloned.1.call-done = (f32[64,2816]{1,0:T(8,128)}, f32[64,2816]{1,0:T(8,128)}) async-done(((f32[64,2816]{1,0:T(8,128)}, f32[64,2816]{1,0:T(8,128)}), (f32[64,2816]{1,0:T(8,128)}, f32[64,2816]{1,0:T(8,128)})) %all-reduce.8.cloned.1.call-update) | async-done | bytes 1441808 | tf_op jit(solution)/shard_map/psum | solution.py:30
  545.1 3.6 fusion.1
  549.9 17.6 %reduce-scatter.20.cloned.1.call-done = f32[64,128]{1,0:T(8,128)} async-done(((f32[64,512]{1,0:T(8,128)}), f32[64,128]{1,0:T(8,128)}) %reduce-scatter.20.cloned.1.call-update) | async-done | bytes 32784 | tf_op jit(solution)/shard_map/reduce_scatter | solution.py:23
  (94 shorter events, 22.2 us)
Async XLA Ops:
  7.2 7.3 %copy-start = (bf16[512,2816]{1,0:T(8,128)(2,1)S(1)}, bf16[512,2816]{1,0:T(8,128)(2,1)}, u32[]{:S(2)}) copy-start(bf16[512,2816]{1,0:T(8,128)(2,1)} %param.30) | copy-start | bytes 8650756
  7.2 99.2 %all-reduce.10.cloned.1.call-start = ((), (), s32[]{:S(2)}) async-start(), calls=%async_computation.15 | async-start | bytes 2883584 | tf_op jit(solution)/shard_map/psum | solution.py:30
  7.2 8.7 %copy-start.1 = (bf16[512,2816]{1,0:T(8,128)(2,1)S(1)}, bf16[512,2816]{1,0:T(8,128)(2,1)}, u32[]{:S(2)}) copy-start(bf16[512,2816]{1,0:T(8,128)(2,1)} %param.29) | copy-start | bytes 8650756
  17.5 111.5 %reduce-scatter.8.cloned.1.call-start = ((), (), s32[]{:S(2)}) async-start(), calls=%async_computation.7 | async-start | bytes 163840 | tf_op jit(solution)/shard_map/reduce_scatter | solution.py:23
  106.4 3.7 copy-start.12
  106.4 22.6 %copy-start.7 = (bf16[64,128]{1,0:T(8,128)(2,1)S(1)}, bf16[64,128]{1,0:T(8,128)(2,1)}, u32[]{:S(2)}) copy-start(bf16[64,128]{1,0:T(8,128)(2,1)} %param.27) | copy-start | bytes 49156
  106.4 28.6 %copy-start.3 = (bf16[512,512]{1,0:T(8,128)(2,1)S(1)}, bf16[512,512]{1,0:T(8,128)(2,1)}, u32[]{:S(2)}) copy-start(bf16[512,512]{1,0:T(8,128)(2,1)} %param.35) | copy-start | bytes 1572868
  110.0 32.2 %copy-start.9 = (bf16[4,512]{1,0:T(4,128)(2,1)S(1)}, bf16[4,512]{1,0:T(4,128)(2,1)}, u32[]{:S(2)}) copy-start(bf16[4,512]{1,0:T(4,128)(2,1)} %param.42) | copy-start | bytes 12292
  110.0 32.2 %copy-start.10 = (bf16[4,512]{1,0:T(4,128)(2,1)S(1)}, bf16[4,512]{1,0:T(4,128)(2,1)}, u32[]{:S(2)}) copy-start(bf16[4,512]{1,0:T(4,128)(2,1)} %param.43) | copy-start | bytes 12292
  110.0 33.7 %copy-start.11 = (bf16[2048]{0:T(1024)(128)(2,1)S(1)}, bf16[2048]{0:T(1024)(128)(2,1)}, u32[]{:S(2)}) copy-start(bf16[2048]{0:T(1024)(128)(2,1)} %param.48) | copy-start | bytes 12292
  110.1 87.8 %reduce-scatter.12.cloned.1.call-start = ((), (), s32[]{:S(2)}) async-start(), calls=%async_computation.9 | async-start | bytes 147456 | tf_op jit(solution)/shard_map/reduce_scatter | solution.py:125
  135.9 126.2 %reduce-scatter.14.cloned.1.call-start = ((), (), s32[]{:S(2)}) async-start(), calls=%async_computation.10 | async-start | bytes 147456 | tf_op jit(solution)/shard_map/reduce_scatter | solution.py:126
  137.8 49.9 %copy-start.14 = (f32[32]{0:T(128)S(1)}, f32[32]{0:T(128)}, u32[]{:S(2)}) copy-start(f32[32]{0:T(128)} %param.38) | copy-start | bytes 388
  137.9 125.0 %copy-start.5 = (bf16[8,3,512]{2,0,1:T(8,128)(2,1)S(1)}, bf16[8,3,512]{2,0,1:T(8,128)(2,1)}, u32[]{:S(2)}) copy-start(bf16[8,3,512]{2,0,1:T(8,128)(2,1)} %param.46) | copy-start | bytes 73732
  137.9 125.0 %copy-start.6 = (bf16[8,3,512]{2,0,1:T(8,128)(2,1)S(1)}, bf16[8,3,512]{2,0,1:T(8,128)(2,1)}, u32[]{:S(2)}) copy-start(bf16[8,3,512]{2,0,1:T(8,128)(2,1)} %param.45) | copy-start | bytes 73732
  137.9 189.5 %reduce-scatter.10.cloned.1.call-start = ((), (), s32[]{:S(2)}) async-start(), calls=%async_computation.8 | async-start | bytes 589824 | tf_op jit(solution)/shard_map/reduce_scatter | solution.py:124
  140.8 187.5 %copy-start.4 = (bf16[8,3,2048]{2,0,1:T(8,128)(2,1)S(1)}, bf16[8,3,2048]{2,0,1:T(8,128)(2,1)}, u32[]{:S(2)}) copy-start(bf16[8,3,2048]{2,0,1:T(8,128)(2,1)} %param.44) | copy-start | bytes 294916
  140.8 251.8 %reduce-scatter.16.cloned.1.call-start = ((), (), s32[]{:S(2)}) async-start(), calls=%async_computation.11 | async-start | bytes 589824 | tf_op jit(solution)/shard_map/reduce_scatter | solution.py:123
  184.8 143.6 %copy-start.8 = (f32[8]{0:T(128)}, f32[8]{0:T(128)S(1)}, u32[]{:S(2)}) copy-start(f32[8]{0:T(128)S(1)} %fusion.42) | copy-start | bytes 100
  187.7 259.3 %reduce-scatter.18.cloned.1.call-start = ((), (), s32[]{:S(2)}) async-start(), calls=%async_computation.12 | async-start | bytes 163840 | tf_op jit(solution)/shard_map/reduce_scatter | solution.py:23
  338.6 89.6 %copy-start.13 = (bf16[512]{0:T(512)(128)(2,1)S(1)}, bf16[512]{0:T(512)(128)(2,1)}, u32[]{:S(2)}) copy-start(bf16[512]{0:T(512)(128)(2,1)} %param.50) | copy-start | bytes 3076
  428.1 116.9 %all-reduce.8.cloned.1.call-start = ((), (), s32[]{:S(2)}) async-start(), calls=%async_computation.14 | async-start | bytes 2883584 | tf_op jit(solution)/shard_map/psum | solution.py:30
  446.9 9.5 %copy-start.2 = (bf16[512,2816]{1,0:T(8,128)(2,1)S(1)}, bf16[512,2816]{1,0:T(8,128)(2,1)}, u32[]{:S(2)}) copy-start(bf16[512,2816]{1,0:T(8,128)(2,1)} %param.51) | copy-start | bytes 8650756
  457.9 109.7 %reduce-scatter.20.cloned.1.call-start = ((), (), s32[]{:S(2)}) async-start(), calls=%async_computation.13 | async-start | bytes 163840 | tf_op jit(solution)/shard_map/reduce_scatter | solution.py:23
Sparse Core Ops, SparseCore 0:
  17.6 88.7 all-reduce.9
  110.2 18.7 reduce-scatter.7
  136.0 61.8 reduce-scatter.11
  201.1 60.9 reduce-scatter.13
  265.8 61.5 reduce-scatter.9
  330.6 62.0 reduce-scatter.15
  428.3 18.6 reduce-scatter.17
  458.0 86.9 all-reduce.7
  548.8 18.7 reduce-scatter.19
where the time goes:
time: 576 us; the launch traced here: 575 us
  waiting for transfers between devices  378 us (66%)
  blocking collectives  130 us (23%)
  matrix products  27 us (5%)
  other arithmetic  21.2 us (4%)
  between operations  14.7 us (3%)
    psum x2, waiting for transfers between devices, half_channel(): gate_sum, up_sum, totals = lax.psum((gate_part, up_part, squares), 'kv')  131 us
    reduce_scatter x1, waiting for transfers between devices, local(): lax.psum_scatter(value_part, 'kv', scatter_dimension=0, tiled=True)  64.4 us
    reduce_scatter x1, waiting for transfers between devices, local(): lax.psum_scatter(read_part, 'kv', scatter_dimension=0, tiled=True)  64.1 us
    reduce_scatter x3, waiting for transfers between devices, column_sums(): lax.psum_scatter(partial_terms, 'tp', scatter_dimension=1, tiled=True)  55.2 us
    reduce_scatter x1, waiting for transfers between devices, local(): lax.psum_scatter(gate_part, 'kv', scatter_dimension=0, tiled=True)  53.9 us
    psum x2, blocking collectives, half_channel(): gate_sum, up_sum, totals = lax.psum((gate_part, up_part, squares), 'kv')  44.8 us
    unnamed x1, blocking collectives  37.5 us
    all_gather x1, blocking collectives, local(): lax.all_gather(mixer_rows, 'kv', axis=0, tiled=True)  30.9 us
  transfers between devices with their start and end apart: 9, of which 9 were waited for; matrix products, arithmetic and copies ran while one was open for 5% of the time, Pallas kernels for 0%

commit v1 on v0

--- a/solution.py
+++ b/solution.py
@@ -1,6 +1,10 @@
+import functools
+
 import jax
 import jax.numpy as jnp
 from jax import lax
+from jax.experimental import pallas as pl
+from jax.experimental.pallas import tpu as pltpu
 from jax.sharding import PartitionSpec as P
 
 D = 4096
@@ -10,29 +14,334 @@
 
 EPS = 1e-06
 
-
-def lifted_rows(current, gain_vec):
-    gathered = lax.all_gather(current, "tp", axis=1, tiled=True)
-    widened = gathered.astype(jnp.float32)
+MESH = pl.DeviceIdType.MESH
+
+
+def greet(axis, n, me):
+    barrier = pltpu.get_barrier_semaphore()
+    for d in range(1, n):
+        pl.semaphore_signal(
+            barrier, inc=1, device_id={axis: lax.rem(me + d, n)}, device_id_type=MESH
+        )
+    pl.semaphore_wait(barrier, n - 1)
+
+
+def start_scatter(axis, n, me, parts, landed, send_sem, recv_sem):
+    copies = []
+    for d in range(1, n):
+        peer = lax.rem(me + d, n)
+        for k, (src, dst) in enumerate(zip(parts, landed)):
+            copy = pltpu.make_async_remote_copy(
+                src_ref=src.at[peer],
+                dst_ref=dst.at[d],
+                send_sem=send_sem.at[k, d],
+                recv_sem=recv_sem.at[k, d],
+                device_id={axis: peer},
+                device_id_type=MESH,
+            )
+            copy.start()
+            copies.append(copy)
+    return copies
+
+
+def start_gather(axis, n, me, rows, send_sem, recv_sem):
+    copies = []
+    for d in range(1, n):
+        copy = pltpu.make_async_remote_copy(
+            src_ref=rows.at[me],
+            dst_ref=rows.at[me],
+            send_sem=send_sem.at[d],
+            recv_sem=recv_sem.at[d],
+            device_id={axis: lax.rem(me + d, n)},
+            device_id_type=MESH,
+        )
+        copy.start()
+        copies.append(copy)
+    return copies
+
+
+def finish(copies):
+    for copy in copies:
+        copy.wait_recv()
+    for copy in copies:
+        copy.wait_send()
+
+
+def summed(n, me, own, landed):
+    total = own[me].astype(jnp.float32)
+    for d in range(1, n):
+        total = total + landed[d].astype(jnp.float32)
+    return total
+
+
+def greet_pairs(axis, n, me):
+    barrier = pltpu.get_barrier_semaphore()
+    pair, _, lines = places(n, me)
+    for peer in [pair] + lines[1:]:
+        pl.semaphore_signal(barrier, inc=1, device_id={axis: peer}, device_id_type=MESH)
+    pl.semaphore_wait(barrier, n // 2)
+
+
+def places(n, me):
+    side, spot, m = lax.rem(me, 2), me // 2, n // 2
+    steps = [lax.rem(spot + e, m) for e in range(m)]
+    return me + 1 - 2 * side, [2 * q + 1 - side for q in steps], [2 * q + side for q in steps]
+
+
+def remote(src, dst, send_sem, recv_sem, axis, peer):
+    return pltpu.make_async_remote_copy(
+        src_ref=src,
+        dst_ref=dst,
+        send_sem=send_sem,
+        recv_sem=recv_sem,
+        device_id={axis: peer},
+        device_id_type=MESH,
+    )
+
+
+def pair_scatter(axis, n, me, parts, staged, partial, landed, sems):
+    pair_send, pair_recv, line_send, line_recv = sems
+    pair, across, lines = places(n, me)
+    m = n // 2
+    first, second = {}, {}
+    for k, part in enumerate(parts):
+        for e in list(range(1, m)) + [0]:
+            first[k, e] = remote(
+                part.at[across[e]], staged[k].at[e], pair_send.at[k, e], pair_recv.at[k, e],
+                axis, pair,
+            )
+            first[k, e].start()
+    for k, part in enumerate(parts):
+        for e in range(1, m):
+            first[k, e].wait_recv()
+            both = part[lines[e]].astype(jnp.float32) + staged[k][e].astype(jnp.float32)
+            partial[k][e] = both.astype(part.dtype)
+            second[k, e] = remote(
+                partial[k].at[e], landed[k].at[e], line_send.at[k, e], line_recv.at[k, e],
+                axis, lines[e],
+            )
+            second[k, e].start()
+    totals = []
+    for k, part in enumerate(parts):
+        first[k, 0].wait_recv()
+        total = part[me].astype(jnp.float32) + staged[k][0].astype(jnp.float32)
+        for e in range(1, m):
+            second[k, e].wait_recv()
+            total = total + landed[k][e].astype(jnp.float32)
+        totals.append(total)
+    return totals, list(first.values()) + list(second.values())
+
+
+def pair_gather(axis, n, me, rows, sems):
+    pair_send, pair_recv, line_send, line_recv = sems
+    pair, _, lines = places(n, me)
+    m = n // 2
+    side = lax.rem(me, 2)
+    sends = []
+    own = rows.at[me]
+    for e in range(1, m):
+        copy = remote(own, own, line_send.at[e], line_recv.at[e], axis, lines[e])
+        copy.start()
+        sends.append(copy)
+    copy = remote(own, own, pair_send.at[0], pair_recv.at[0], axis, pair)
+    copy.start()
+    passed = [copy]
+    for e in range(1, m):
+        sends[e - 1].wait_recv()
+        came = rows.at[2 * lax.rem(me // 2 + m - e, m) + side]
+        copy = remote(came, came, pair_send.at[e], pair_recv.at[e], axis, pair)
+        copy.start()
+        passed.append(copy)
+    for copy in passed:
+        copy.wait_recv()
+    for copy in sends + passed:
+        copy.wait_send()
+
+
+def gather_kernel(axis, n, own, rows, send_sem, recv_sem):
+    me = lax.axis_index(axis)
+    rows[me] = own[...]
+    greet(axis, n, me)
+    finish(start_gather(axis, n, me, rows, send_sem, recv_sem))
+
+
+def pair_gather_kernel(axis, n, own, rows, *sems):
+    me = lax.axis_index(axis)
+    rows[me] = own[...]
+    greet_pairs(axis, n, me)
+    pair_gather(axis, n, me, rows, sems)
+
+
+def scatter_kernel(axis, n, count, *refs):
+    parts, outs, staged, partial, landed = (
+        refs[k * count : (k + 1) * count] for k in range(5)
+    )
+    me = lax.axis_index(axis)
+    greet_pairs(axis, n, me)
+    totals, copies = pair_scatter(
+        axis, n, me, parts, staged, partial, landed, refs[5 * count :]
+    )
+    for out, total in zip(outs, totals):
+        out[...] = total
+    for copy in copies:
+        copy.wait_send()
+
+
+def hidden_kernel(axis, n, squares, gate, up, rows, *refs):
+    me = lax.axis_index(axis)
+    greet_pairs(axis, n, me)
+    (square_sum, gate_sum, up_sum), copies = pair_scatter(
+        axis, n, me, (squares, gate, up), refs[:3], refs[3:6], refs[6:9], refs[9:13]
+    )
+    row_scale = lax.rsqrt(square_sum[:, :1] / D + EPS)
+    gate_sum = gate_sum * row_scale
+    up_sum = up_sum * row_scale
+    rows[me] = (gate_sum / (1.0 + jnp.exp(-gate_sum)) * up_sum).astype(rows.dtype)
+    pair_gather(axis, n, me, rows, refs[13:])
+    for copy in copies:
+        copy.wait_send()
+
+
+def add_kernel(
+    axis, n, weight, terms, base, gain, rows, lifted, squares,
+    terms_in, send_sem, recv_sem, rows_send, rows_recv,
+):
+    me = lax.axis_index(axis)
+    greet(axis, n, me)
+    copies = start_scatter(axis, n, me, (terms,), (terms_in,), send_sem, recv_sem)
+    for copy in copies:
+        copy.wait_recv()
+    returned = summed(n, me, terms, terms_in)
+    rows[me] = (base[me].astype(jnp.float32) + weight * returned).astype(rows.dtype)
+    gathers = start_gather(axis, n, me, rows, rows_send, rows_recv)
+    for copy in copies:
+        copy.wait_send()
+    finish(gathers)
+    for k in range(n):
+        widened = rows[k].astype(jnp.float32)
+        lifted[k] = (widened * gain[...].astype(jnp.float32)).astype(lifted.dtype)
+        total = jnp.sum(widened * widened, axis=1, keepdims=True)
+        squares[k] = jnp.broadcast_to(total, squares.shape[1:])
+
+
+def call(kernel, args, outs, scratch, ident, micros):
+    vmem = pl.BlockSpec(memory_space=pltpu.VMEM)
+    return pl.pallas_call(
+        kernel,
+        out_shape=outs,
+        in_specs=[vmem] * len(args),
+        out_specs=jax.tree.map(lambda _: vmem, outs),
+        scratch_shapes=scratch,
+        compiler_params=pltpu.CompilerParams(
+            collective_id=ident, has_side_effects=True, vmem_limit_bytes=8 * 2**20
+        ),
+        cost_estimate=pl.CostEstimate(
+            flops=0, bytes_accessed=micros * 3_000_000, transcendentals=0
+        ),
+    )(*args)
+
+
+def sems(count, *shape):
+    return [pltpu.SemaphoreType.DMA(shape)] * count
+
+
+def gathered(own, axis, ident):
+    n = lax.axis_size(axis)
+    return call(
+        functools.partial(gather_kernel, axis, n),
+        (own,),
+        jax.ShapeDtypeStruct((n,) + own.shape, own.dtype),
+        sems(2, n),
+        ident,
+        4,
+    )
+
+
+def gathered_pairs(own, axis, ident):
+    n = lax.axis_size(axis)
+    return call(
+        functools.partial(pair_gather_kernel, axis, n),
+        (own,),
+        jax.ShapeDtypeStruct((n,) + own.shape, own.dtype),
+        sems(4, n // 2),
+        ident,
+        8,
+    )
+
+
+def slots(parts, n):
+    return [pltpu.VMEM((n // 2,) + part.shape[1:], part.dtype) for part in parts] * 3
+
+
+def scattered(parts, axis, ident):
+    n = lax.axis_size(axis)
+    outs = tuple(jax.ShapeDtypeStruct(part.shape[1:], jnp.float32) for part in parts)
+    return call(
+        functools.partial(scatter_kernel, axis, n, len(parts)),
+        parts,
+        outs,
+        slots(parts, n) + sems(4, len(parts), n // 2),
+        ident,
+        14,
+    )
+
+
+def hidden_rows(gate, up, squares, axis, ident):
+    n = lax.axis_size(axis)
+    return call(
+        functools.partial(hidden_kernel, axis, n),
+        (squares, gate, up),
+        jax.ShapeDtypeStruct(gate.shape, gate.dtype),
+        slots((squares, gate, up), n) + sems(4, 3, n // 2) + sems(4, n // 2),
+        ident,
+        24,
+    )
+
+
+def add_rows(terms, base, weight, gain_vec, axis, ident):
+    n = lax.axis_size(axis)
+    shape = (n, base.shape[0] // n, base.shape[1])
+    rows, lifted, squares = call(
+        functools.partial(add_kernel, axis, n, weight),
+        (terms.reshape(shape), base.reshape(shape), gain_vec.reshape(1, -1)),
+        (
+            jax.ShapeDtypeStruct(shape, base.dtype),
+            jax.ShapeDtypeStruct(shape, base.dtype),
+            jax.ShapeDtypeStruct(shape[:2] + (128,), jnp.float32),
+        ),
+        [pltpu.VMEM(shape, terms.dtype)] + sems(2, 1, n) + sems(2, n),
+        ident,
+        7,
+    )
+    return (
+        rows.reshape(base.shape),
+        lifted.reshape(base.shape),
+        squares.reshape(base.shape[0], 128),
+    )
+
+
+def lifted_rows(rows, gain_vec):
+    widened = rows.astype(jnp.float32)
     squares = jnp.sum(widened * widened, axis=1)
     lifted = (widened * gain_vec.astype(jnp.float32)[None, :]).astype(jnp.bfloat16)
-    return (lifted, squares)
-
-
-def column_sums(partial_terms):
-    return lax.psum_scatter(partial_terms, "tp", scatter_dimension=1, tiled=True)
-
-
-def half_channel(current, gain_vec, gate_weight, up_weight, down_weight):
-    lifted, squares = lifted_rows(current, gain_vec)
-    gate_part = jnp.dot(lifted, gate_weight, preferred_element_type=jnp.float32)
-    up_part = jnp.dot(lifted, up_weight, preferred_element_type=jnp.float32)
-    gate_sum, up_sum, totals = lax.psum((gate_part, up_part, squares), "kv")
-    row_scale = lax.rsqrt(totals / D + EPS)[:, None]
-    hidden = (jax.nn.silu(gate_sum * row_scale) * (up_sum * row_scale)).astype(jnp.bfloat16)
-    down_sum = jnp.dot(hidden, down_weight, preferred_element_type=jnp.float32)
-    returned = column_sums(down_sum)
-    return (current.astype(jnp.float32) + 0.5 * returned).astype(jnp.bfloat16)
+    return (lifted, jnp.broadcast_to(squares[:, None], (squares.shape[0], 128)))
+
+
+def by_rows(array, n):
+    return array.reshape(n, array.shape[0] // n, array.shape[1])
+
+
+def product(rows, weight):
+    return jnp.dot(rows, weight, preferred_element_type=jnp.float32)
+
+
+def half_channel(rows, lifted, squares, gate_weight, up_weight, down_weight, next_gain, ident):
+    n = lax.axis_size("kv")
+    gate_part = by_rows(product(lifted, gate_weight).astype(jnp.bfloat16), n)
+    up_part = by_rows(product(lifted, up_weight).astype(jnp.bfloat16), n)
+    hidden = hidden_rows(gate_part, up_part, by_rows(squares, n), "kv", ident)
+    hidden = hidden.reshape(rows.shape[0], hidden.shape[2])
+    return add_rows(product(hidden, down_weight), rows, 0.5, next_gain, "tp", ident + 1)
 
 
 def short_conv(window_state, fresh, taps):
@@ -112,21 +421,24 @@
     after_up,
     after_down,
 ):
-    first_out = half_channel(block_in, before_gain, before_gate, before_up, before_down)
-    lifted, squares = lifted_rows(first_out, mix_gain)
-    gate_part = jnp.dot(lifted, input_gate, preferred_element_type=jnp.float32)
-    value_part = jnp.dot(lifted, input_value, preferred_element_type=jnp.float32)
-    write_part = jnp.dot(lifted, input_write, preferred_element_type=jnp.float32)
-    read_part = jnp.dot(lifted, input_read, preferred_element_type=jnp.float32)
-    step_part = jnp.dot(lifted, input_step, preferred_element_type=jnp.float32)
-    gate_sum, value_sum, write_sum, read_sum, step_sum, totals = (
-        lax.psum_scatter(gate_part, "kv", scatter_dimension=0, tiled=True),
-        lax.psum_scatter(value_part, "kv", scatter_dimension=0, tiled=True),
-        lax.psum_scatter(write_part, "kv", scatter_dimension=0, tiled=True),
-        lax.psum_scatter(read_part, "kv", scatter_dimension=0, tiled=True),
-        lax.psum_scatter(step_part, "kv", scatter_dimension=0, tiled=True),
-        lax.psum_scatter(squares, "kv", scatter_dimension=0, tiled=True),
-    )
+    n = lax.axis_size("kv")
+    blocks = gathered(block_in, "tp", 0)
+    start = blocks.transpose(1, 0, 2).reshape(blocks.shape[1], -1)
+    first_out, lifted, squares = half_channel(
+        start, *lifted_rows(start, before_gain), before_gate, before_up, before_down, mix_gain, 1
+    )
+    parts = [
+        by_rows(product(lifted, weight).astype(jnp.bfloat16), n)
+        for weight in (input_gate, input_value, input_write, input_read)
+    ]
+    heads = input_step.shape[1]
+    step_weight = jnp.pad(input_step, ((0, 0), (0, -heads % 128)))
+    square_sum, gate_sum, value_sum, write_sum, read_sum, step_sum = scattered(
+        (by_rows(squares, n),) + tuple(parts) + (by_rows(product(lifted, step_weight), n),),
+        "kv",
+        3,
+    )
+    step_sum, totals = step_sum[:, :heads], square_sum[:, 0]
     mix_scale = lax.rsqrt(totals / D + EPS)[:, None]
     gate_rows = (gate_sum * mix_scale).astype(jnp.bfloat16)
     value_fresh = (value_sum * mix_scale).astype(jnp.bfloat16)
@@ -148,14 +460,14 @@
         scan_state,
     )
     mixer_rows = (normed * group_gain.astype(jnp.float32)[None, :]).astype(jnp.bfloat16)
-    back_part = jnp.dot(
-        lax.all_gather(mixer_rows, "kv", axis=0, tiled=True),
-        mixer_out,
-        preferred_element_type=jnp.float32,
-    )
-    returned = column_sums(back_part)
-    middle = (first_out.astype(jnp.float32) + returned).astype(jnp.bfloat16)
-    block_out = half_channel(middle, after_gain, after_gate, after_up, after_down)
+    mixer_all = gathered_pairs(mixer_rows, "kv", 4)
+    back_part = product(mixer_all.reshape(-1, mixer_all.shape[2]), mixer_out)
+    middle, lifted, squares = add_rows(back_part, first_out, 1.0, after_gain, "tp", 5)
+    last, _, _ = half_channel(
+        middle, lifted, squares, after_gate, after_up, after_down, after_gain, 6
+    )
+    width = block_in.shape[1]
+    block_out = lax.dynamic_slice_in_dim(last, lax.axis_index("tp") * width, width, 1)
     return (block_out, state_next, value_next, write_next, read_next)
 
 

time: 576 us -> 144 us (0.25)
  waiting for transfers between devices: 378 us -> 0 us
  blocking collectives: 130 us -> 0 us
  Pallas kernels: 0 us -> 102 us
  matrix products: 27 us -> 13.1 us
  between operations: 14.7 us -> 1.1 us
  local copies, waits for them, and re-layouts: 3.67 us -> 9.51 us
    reduce_scatter x7 -> x0, waiting for transfers between devices: 247 us -> none  [the longest x1 64.4 us: local(): lax.psum_scatter(value_part, 'kv', scatter_dimension=0, tiled=True)]
    psum x2 -> x0, waiting for transfers between devices: 131 us -> none  [half_channel(): gate_sum, up_sum, totals = lax.psum((gate_part, up_part, squares), 'kv')]
    pallas_call x0 -> x8, Pallas kernels: none -> 102 us  [call(): pl.pallas_call(kernel, out_shape=outs, in_specs=[vmem] * len(args), out_s...]
    all_gather x4 -> x0, blocking collectives: 48 us -> none  [the longest x1 30.9 us: local(): lax.all_gather(mixer_rows, 'kv', axis=0, tiled=True)]
    psum x2 -> x0, blocking collectives: 44.8 us -> none  [half_channel(): gate_sum, up_sum, totals = lax.psum((gate_part, up_part, squares), 'kv')]
    unnamed x1 -> x0, blocking collectives: 37.5 us -> none
    dot_general x12, matrix products: 27 us -> 13.1 us  [product(): return jnp.dot(rows, weight, preferred_element_type=jnp.float32)]
    unnamed x31 -> x51, local copies, waits for them, and re-layouts: 1.31 us -> 7.53 us
  transfers between devices with their start and end apart: 9 -> 0, of which waited for: 9 -> 0; matrix products, arithmetic and copies ran while one was open for 5% -> 0% of each run, Pallas kernels for 0% -> 0%
where the time goes in v1:
time: 144 us; the launch traced here: 143 us
  Pallas kernels  102 us (71%)
  other arithmetic  17.3 us (12%)
  matrix products  13.1 us (9%)
  local copies, waits for them, and re-layouts  9.51 us (7%)
    pallas_call x8, Pallas kernels, call(): pl.pallas_call(kernel, out_shape=outs, in_specs=[vmem] * len(args), out_s...  102 us
    dot_general x12, matrix products, product(): return jnp.dot(rows, weight, preferred_element_type=jnp.float32)  13.1 us
    reduce_sum x1, other arithmetic, state_update(): jnp.sum(state_next * read_heads[:, :, None, :], axis=3)  9.38 us
    unnamed x51, local copies, waits for them, and re-layouts  7.53 us

profile of v1, /device:TPU:0, one launch (start us, length us, event | category | flops | bytes accessed | tf_op | source)
XLA Modules:
  0.0 142.8 jit_solution(4552695971052046234)
XLA Ops:
  0.7 0.9 copy-done.9
  1.5 4.9 %shard_map.290 = bf16[4,64,128]{2,1,0:T(8,128)(2,1)S(1)} custom-call(bf16[64,128]{1,0:T(8,128)(2,1)S(1)} %copy-done.9), custom_call_target="tpu_custom_call" | custom-call | bytes 12000000 | tf_op jit(solution)/shard_map/pallas_call | solution.py:229
  7.8 1.3 fusion.1.up
  9.4 1.0 copy-done.1
  10.4 26.1 %shard_map.291 = bf16[8,8,2816]{2,1,0:T(8,128)(2,1)S(1)} custom-call(f32[8,8,128]{2,1,0:T(8,128)S(1)} %broadcast_in_dim.15.squares, bf16[8,8,2816]{2,1,0:T(8,128)(2,1)S(1)} %fusion.gate, bf16[8,8,2816]{2,1,0:T(8,128)(2,1)S(1)} %copy-done.1), custom_call_target="tpu_custom_call" | custom-call | bytes 72000000 | tf_op jit(solution)/shard_map/pallas_call | solution.py:229
  36.5 2.4 %fusion.6.terms = f32[4,16,512]{2,1,0:T(8,128)S(1)} fusion(bf16[4,16,2816]{2,1,0:T(8,128)(2,1)S(1)} %bitcast.86, bf16[2816,512]{1,0:T(8,128)(2,1)} %param.31), kind=kOutput, calls=%fused_computation.12 | convolution fusion | flops 184549376 | bytes 3375104 | tf_op jit(solution)/shard_map/dot_general | solution.py:335
  39.1 7.5 %shard_map.292 = (bf16[4,16,512]{2,1,0:T(8,128)(2,1)S(1)}, bf16[4,16,512]{2,1,0:T(8,128)(2,1)S(1)}, f32[4,16,128]{2,1,0:T(8,128)S(1)}) custom-call(f32[4,16,512]{2,1,0:T(8,128)S(1)} %fusion.6.terms, bf16[4,16,512]{2,1,0:T(8,128)(2,1)S(1)} %reshape_reshape.9.base, bf16[1,512]{1,0:T(2,128)(2,1)S(1)} %reshape.145.gain), custom_call_target="tpu_custom_call" | custom-call | bytes 21000000 | tf_op jit(solution)/shard_map/pallas_call | solution.py:229
  47.8 2.1 %fusion.8.refs_1_ = bf16[8,8,2048]{2,1,0:T(8,128)(2,1)S(1)} fusion(bf16[64,512]{1,0:T(8,128)(2,1)S(1)} %bitcast.88, bf16[512,2048]{1,0:T(8,128)(2,1)} %param.33), kind=kOutput, calls=%fused_computation.16 | convolution fusion | flops 134348800 | bytes 2424832 | tf_op jit(solution)/shard_map/dot_general | solution.py:335
  50.6 0.8 fusion.13.refs_4_
  51.5 1.5 %copy.36 = bf16[512,32]{1,0:T(8,128)(2,1)} copy(bf16[512,32]{0,1:T(8,128)(2,1)} %param.37) | data formatting | bytes 65536 | tf_op args[10]
  53.0 1.1 fusion.16.refs_5_
  54.0 0.8 copy-done.2
  54.9 0.8 copy-done.8
  55.6 15.9 %shard_map.293 = (f32[8,128]{1,0:T(8,128)S(1)}, f32[8,2048]{1,0:T(8,128)S(1)}, f32[8,2048]{1,0:T(8,128)S(1)}, f32[8,512]{1,0:T(8,128)S(1)}, f32[8,512]{1,0:T(8,128)S(1)}, /*index=5*/f32[8,128]{1,0:T(8,128)S(1)}) custom-call(f32[8,8,128]{2,1,0:T(8,128)S(1)} %bitcast.97, bf16[8,8,2048]{2,1,0:T(8,128)(2,1)S(1)} %fusion.8.refs_1_, ...), custom_call_target="tpu_custom_call" | custom-call | bytes 42000000 | tf_op jit(solution)/shard_map/pallas_call | solution.py:229
  73.6 0.7 multiply_exponential_fusion
  75.2 0.9 multiply_reduce_fusion.1
  76.3 0.8 fusion.29
  78.5 0.8 multiply_reduce_fusion.2
  79.4 9.4 %multiply_reduce_fusion = (f32[8,32,64]{2,1,0:T(8,128)S(1)}, f32[8,32,64,128]{3,2,1,0:T(8,128)}) fusion(f32[8,32,128]{2,1,0:T(8,128)S(1)} %broadcast_bitcast_fusion, f32[8,32,128]{2,1,0:T(8,128)S(1)} %broadcast_bitcast_fusion.1, f32[8,32,64]{2,1,0:T(8,128)S(1)} %multiply_multiply_fusion, f32[8,32,64,128]{3,2,1,0:T(8,128)} %param.47, ...), kind=kLoop, calls=%fused_computation | loop fusion | flops 10469376 | bytes 17171456 | tf_op jit(solution)/shard_map/reduce_sum | solution.py:385
  89.4 9.2 %shard_map.294 = bf16[8,8,2048]{2,1,0:T(8,128)(2,1)S(1)} custom-call(bf16[8,2048]{1,0:T(8,128)(2,1)S(1)} %multiply_convert_fusion.own), custom_call_target="tpu_custom_call" | custom-call | bytes 24000000 | tf_op jit(solution)/shard_map/pallas_call | solution.py:229
  98.6 2.2 %fusion.10.terms = f32[4,16,512]{2,1,0:T(8,128)S(1)} fusion(bf16[4,16,2048]{2,1,0:T(8,128)(2,1)S(1)} %bitcast.94, bf16[2048,512]{1,0:T(8,128)(2,1)} %param.49), kind=kOutput, calls=%fused_computation.18 | convolution fusion | flops 134217728 | bytes 2490368 | tf_op jit(solution)/shard_map/dot_general | solution.py:335
  100.8 6.6 %shard_map.295 = (bf16[4,16,512]{2,1,0:T(8,128)(2,1)S(1)}, bf16[4,16,512]{2,1,0:T(8,128)(2,1)S(1)}, f32[4,16,128]{2,1,0:T(8,128)S(1)}) custom-call(f32[4,16,512]{2,1,0:T(8,128)S(1)} %fusion.10.terms, bf16[4,16,512]{2,1,0:T(8,128)(2,1)S(1)} %copy-done.4, bf16[1,512]{1,0:T(2,128)(2,1)S(1)} %reshape.151.gain), custom_call_target="tpu_custom_call" | custom-call | bytes 21000000 | tf_op jit(solution)/shard_map/pallas_call | solution.py:229
  108.7 23.4 %shard_map.296 = bf16[8,8,2816]{2,1,0:T(8,128)(2,1)S(1)} custom-call(f32[8,8,128]{2,1,0:T(8,128)S(1)} %bitcast.98, bf16[8,8,2816]{2,1,0:T(8,128)(2,1)S(1)} %fusion.2.gate, bf16[8,8,2816]{2,1,0:T(8,128)(2,1)S(1)} %fusion.3.up), custom_call_target="tpu_custom_call" | custom-call | bytes 72000000 | tf_op jit(solution)/shard_map/pallas_call | solution.py:229
  132.8 8.1 %shard_map.297 = (bf16[4,16,512]{2,1,0:T(8,128)(2,1)S(1)}, bf16[4,16,512]{2,1,0:T(8,128)(2,1)}, f32[4,16,128]{2,1,0:T(8,128)}) custom-call(f32[4,16,512]{2,1,0:T(8,128)S(1)} %fusion.4.terms, bf16[4,16,512]{2,1,0:T(8,128)(2,1)S(1)} %get-tuple-element.29.base, bf16[1,512]{1,0:T(2,128)(2,1)S(1)} %reshape.151.gain), custom_call_target="tpu_custom_call" | custom-call | bytes 21000000 | tf_op jit(solution)/shard_map/pallas_call | solution.py:229
  (86 shorter events, 12.4 us)
Async XLA Ops:
  0.6 6.5 %copy-start = (bf16[512,2816]{1,0:T(8,128)(2,1)S(1)}, bf16[512,2816]{1,0:T(8,128)(2,1)}, u32[]{:S(2)}) copy-start(bf16[512,2816]{1,0:T(8,128)(2,1)} %param.29) | copy-start | bytes 8650756
  0.6 0.9 copy-start.9
  1.5 6.2 %copy-start.12 = (bf16[512,2816]{1,0:T(8,128)(2,1)S(1)}, bf16[512,2816]{1,0:T(8,128)(2,1)}, u32[]{:S(2)}) copy-start(bf16[512,2816]{1,0:T(8,128)(2,1)} %param.30) | copy-start | bytes 8650756
  9.4 1.0 copy-start.1
  36.5 2.5 %copy-start.22 = (bf16[512]{0:T(512)(128)(2,1)S(1)}, bf16[512]{0:T(512)(128)(2,1)}, u32[]{:S(2)}) copy-start(bf16[512]{0:T(512)(128)(2,1)} %param.32) | copy-start | bytes 3076
  39.0 10.9 %copy-start.15 = (bf16[512,2048]{1,0:T(8,128)(2,1)S(1)}, bf16[512,2048]{1,0:T(8,128)(2,1)}, u32[]{:S(2)}) copy-start(bf16[512,2048]{1,0:T(8,128)(2,1)} %param.34) | copy-start | bytes 6291460
  39.0 11.4 %copy-start.16 = (bf16[512,512]{1,0:T(8,128)(2,1)S(1)}, bf16[512,512]{1,0:T(8,128)(2,1)}, u32[]{:S(2)}) copy-start(bf16[512,512]{1,0:T(8,128)(2,1)} %param.35) | copy-start | bytes 1572868
  39.0 11.6 %copy-start.17 = (bf16[512,512]{1,0:T(8,128)(2,1)S(1)}, bf16[512,512]{1,0:T(8,128)(2,1)}, u32[]{:S(2)}) copy-start(bf16[512,512]{1,0:T(8,128)(2,1)} %param.36) | copy-start | bytes 1572868
  46.6 0.6 copy-start.3
  47.2 0.6 copy-start.7
  54.0 0.8 copy-start.2
  54.9 0.8 copy-start.8
  71.6 0.6 copy-start.5
  79.4 9.5 %copy-start.24 = (f32[32]{0:T(128)S(1)}, f32[32]{0:T(128)}, u32[]{:S(2)}) copy-start(f32[32]{0:T(128)} %param.40) | copy-start | bytes 388
  79.4 9.7 %copy-start.6 = (f32[8,2048]{1,0:T(8,128)S(1)}, f32[8,2048]{1,0:T(8,128)}, u32[]{:S(2)}) copy-start(f32[8,2048]{1,0:T(8,128)} %copy-done.5) | copy-start | bytes 196612
  79.4 9.9 %copy-start.21 = (bf16[2048]{0:T(1024)(128)(2,1)S(1)}, bf16[2048]{0:T(1024)(128)(2,1)}, u32[]{:S(2)}) copy-start(bf16[2048]{0:T(1024)(128)(2,1)} %param.48) | copy-start | bytes 12292
  88.8 12.0 %copy-start.23 = (bf16[512]{0:T(512)(128)(2,1)S(1)}, bf16[512]{0:T(512)(128)(2,1)}, u32[]{:S(2)}) copy-start(bf16[512]{0:T(512)(128)(2,1)} %param.50) | copy-start | bytes 3076
  88.8 12.0 %copy-start.4 = (bf16[4,16,512]{2,1,0:T(8,128)(2,1)S(1)}, bf16[4,16,512]{2,1,0:T(8,128)(2,1)}, u32[]{:S(2)}) copy-start(bf16[4,16,512]{2,1,0:T(8,128)(2,1)} %copy-done.3) | copy-start | bytes 196612
  89.2 18.2 %copy-start.13 = (bf16[512,2816]{1,0:T(8,128)(2,1)S(1)}, bf16[512,2816]{1,0:T(8,128)(2,1)}, u32[]{:S(2)}) copy-start(bf16[512,2816]{1,0:T(8,128)(2,1)} %param.51) | copy-start | bytes 8650756
  98.6 9.5 %copy-start.14 = (bf16[512,2816]{1,0:T(8,128)(2,1)S(1)}, bf16[512,2816]{1,0:T(8,128)(2,1)}, u32[]{:S(2)}) copy-start(bf16[512,2816]{1,0:T(8,128)(2,1)} %param.52) | copy-start | bytes 8650756
  108.1 24.1 %copy-start.11 = (bf16[2816,512]{1,0:T(8,128)(2,1)S(1)}, bf16[2816,512]{1,0:T(8,128)(2,1)}, u32[]{:S(2)}) copy-start(bf16[2816,512]{1,0:T(8,128)(2,1)} %param.53) | copy-start | bytes 8650756
  132.1 9.4 %copy-start.19 = (bf16[8,3,512]{2,0,1:T(8,128)(2,1)S(1)}, bf16[8,3,512]{2,0,1:T(8,128)(2,1)}, u32[]{:S(2)}) copy-start(bf16[8,3,512]{2,0,1:T(8,128)(2,1)} %param.46) | copy-start | bytes 73732
  132.2 9.4 %copy-start.20 = (bf16[8,3,512]{2,0,1:T(8,128)(2,1)S(1)}, bf16[8,3,512]{2,0,1:T(8,128)(2,1)}, u32[]{:S(2)}) copy-start(bf16[8,3,512]{2,0,1:T(8,128)(2,1)} %param.45) | copy-start | bytes 73732
  132.2 10.0 %copy-start.18 = (bf16[8,3,2048]{2,0,1:T(8,128)(2,1)S(1)}, bf16[8,3,2048]{2,0,1:T(8,128)(2,1)}, u32[]{:S(2)}) copy-start(bf16[8,3,2048]{2,0,1:T(8,128)(2,1)} %param.44) | copy-start | bytes 294916
  (1 other events, 0.6 us)
